TPU v7x, 32 devices: a whole 2x2x4 slice. The times are simulated.
32 devices in a mesh: sp: 2 (over x), dp: 16 (over z, y, core).
Axes of the slice: x: 2, y: 2, z: 4, core: 2. Of those that a mesh axis runs over, the one named last changes fastest.
Arguments:
- queries: bfloat16 [16, 384, 16, 128], P('dp', 'sp'), may hold values from -6 to 6
- keys: bfloat16 [16, 384, 16, 128], P('dp', 'sp'), may hold values from -6 to 6
- values: bfloat16 [16, 384, 16, 128], P('dp', 'sp'), may hold values from -6 to 6
- mix_ratio: float32 [16], replicated, may hold values from 0.3 to 0.8
- out_gain: float32 [128], replicated, may hold values from 0.1 to 1.9
- out_weight: bfloat16 [2048, 2048], P(None, 'dp'), may hold values from -0.125 to 0.125
Outputs:
- layer_out: bfloat16 [16, 384, 2048], P('dp', 'sp')
All inputs are finite; a program needn't handle non-finite values.
Results may differ from a plain program's by a relative error of at most 0.0098.
Values may be sent and summed in bfloat16 or wider, within the bound.
A program may use at most 64 MiB of HBM per device.

v0:
```python
import math

import jax
import jax.numpy as jnp
from jax import lax
from jax.sharding import PartitionSpec as P

theta_base = 500000.0
neg_large = -1e30
norm_eps = 1e-05


def rotate_halves(field, positions):
    width = field.shape[-1] // 2
    half = width // 2
    freqs = theta_base ** (-jnp.arange(half, dtype=jnp.float32) * 2.0 / width)
    angle = positions.astype(jnp.float32)[:, None] * freqs[None, :]
    cosine = jnp.cos(angle)[:, None, :]
    sine = jnp.sin(angle)[:, None, :]
    parts = field.reshape(field.shape[0], 2, width)
    lower = parts[..., :half]
    upper = parts[..., half:]
    turned = jnp.concatenate(
        [lower * cosine - upper * sine, upper * cosine + lower * sine], axis=-1
    )
    return turned.reshape(field.shape)


def masked_softmax(scores, visible):
    kept = jnp.where(visible, scores, neg_large)
    highest = jnp.max(kept, axis=-1, keepdims=True)
    powers = jnp.exp(kept - highest)
    return powers / jnp.sum(powers, axis=-1, keepdims=True)


def head_attention(query_head, key_head, value_head, ratio, gain):
    length = query_head.shape[0]
    width = query_head.shape[1] // 2
    positions = jnp.arange(length, dtype=jnp.int32)
    rotated_queries = (
        rotate_halves(query_head.astype(jnp.float32), positions) * width ** (-0.5)
    ).astype(jnp.bfloat16)
    rotated_keys = rotate_halves(key_head.astype(jnp.float32), positions).astype(jnp.bfloat16)
    block = math.gcd(512, length)

    def one_block(start):
        query_rows = lax.dynamic_slice_in_dim(rotated_queries, start, block, 0)
        visible = (start + jnp.arange(block, dtype=jnp.int32))[:, None] >= positions[None, :]
        first = jnp.dot(
            query_rows[:, :width], rotated_keys[:, :width].T, preferred_element_type=jnp.float32
        )
        second = jnp.dot(
            query_rows[:, width:], rotated_keys[:, width:].T, preferred_element_type=jnp.float32
        )
        weights = (masked_softmax(first, visible) - ratio * masked_softmax(second, visible)).astype(
            jnp.bfloat16
        )
        mixed = jnp.dot(weights, value_head, preferred_element_type=jnp.float32)
        scale = lax.rsqrt(jnp.mean(mixed * mixed, axis=-1, keepdims=True) + norm_eps)
        return (mixed * scale * gain).astype(jnp.bfloat16)

    starts = jnp.arange(length // block, dtype=jnp.int32) * block
    return lax.map(one_block, starts).reshape(length, value_head.shape[1])


def on_device(queries, keys, values, mix_ratio, out_gain, out_weight):
    groups = lax.axis_size("sp")
    heads_here = queries.shape[2] // groups
    query_all, key_all, value_all = (
        lax.all_to_all(queries, "sp", split_axis=2, concat_axis=1, tiled=True),
        lax.all_to_all(keys, "sp", split_axis=2, concat_axis=1, tiled=True),
        lax.all_to_all(values, "sp", split_axis=2, concat_axis=1, tiled=True),
    )
    seqs = query_all.shape[0]
    length = query_all.shape[1]
    first_head = lax.axis_index("sp") * heads_here
    ratios = lax.dynamic_slice_in_dim(mix_ratio, first_head, heads_here, 0)
    item_ratios = jnp.tile(ratios, seqs)

    def by_item(field):
        return jnp.swapaxes(field, 1, 2).reshape(seqs * heads_here, length, field.shape[3])

    def one_head(head_items):
        query_head, key_head, value_head, ratio = head_items
        return head_attention(query_head, key_head, value_head, ratio, out_gain)

    heads = lax.map(
        one_head, (by_item(query_all), by_item(key_all), by_item(value_all), item_ratios)
    )
    attended = jnp.swapaxes(heads.reshape(seqs, heads_here, length, heads.shape[2]), 1, 2)
    returned = lax.all_to_all(attended, "sp", split_axis=1, concat_axis=2, tiled=True)
    tokens_here = returned.shape[1]
    token_rows = returned.reshape(seqs * tokens_here, -1)
    result = jnp.dot(
        token_rows,
        lax.all_gather(out_weight, "dp", axis=1, tiled=True),
        preferred_element_type=jnp.float32,
    ).astype(jnp.bfloat16)
    return result.reshape(seqs, tokens_here, -1)


def solution(mesh):
    in_specs = (
        P("dp", "sp", None, None),
        P("dp", "sp", None, None),
        P("dp", "sp", None, None),
        P(),
        P(),
        P(None, "dp"),
    )
    out_specs = P("dp", "sp", None)
    return jax.shard_map(
        on_device, mesh=mesh, in_specs=in_specs, out_specs=out_specs, check_vma=False
    )
```

profile of v0, /device:TPU:0, one launch (start us, length us, event | category | flops | bytes accessed | tf_op | source)
XLA Modules:
  0.0 221.7 jit_solution(10596133892505202635)
XLA Ops:
  6.5 2.2 %copy.37 = bf16[1,192,16,128]{3,1,0,2:T(8,128)(2,1)} copy(bf16[1,192,16,128]{3,2,1,0:T(8,128)(2,1)} %param.10) | data formatting | bytes 1572864 | tf_op args[0]
  8.8 4.2 %all-to-all-start = ((bf16[1,192,16,128]{3,1,0,2:T(8,128)(2,1)}), bf16[1,192,16,128]{3,1,0,2:T(8,128)(2,1)S(1)}, u32[]{:S(2)}, u32[]{:S(2)}) async-start(bf16[1,192,16,128]{3,1,0,2:T(8,128)(2,1)} %copy.37), calls=%async_computation | async-start | bytes 1572864 | tf_op jit(solution)/shard_map/all_to_all | solution.py:70
  13.0 2.2 %copy.40 = bf16[1,192,16,128]{3,1,0,2:T(8,128)(2,1)} copy(bf16[1,192,16,128]{3,2,1,0:T(8,128)(2,1)} %param.11) | data formatting | bytes 1572864 | tf_op args[1]
  15.2 9.3 %all-to-all-done = bf16[1,192,16,128]{3,1,0,2:T(8,128)(2,1)S(1)} async-done(((bf16[1,192,16,128]{3,1,0,2:T(8,128)(2,1)}), bf16[1,192,16,128]{3,1,0,2:T(8,128)(2,1)S(1)}, u32[]{:S(2)}, u32[]{:S(2)}) %all-to-all-start) | async-done | bytes 786464 | tf_op jit(solution)/shard_map/all_to_all | solution.py:70
  24.6 3.5 %all-to-all-start.1 = ((bf16[1,192,16,128]{3,1,0,2:T(8,128)(2,1)}), bf16[1,192,16,128]{3,1,0,2:T(8,128)(2,1)S(1)}, u32[]{:S(2)}, u32[]{:S(2)}) async-start(bf16[1,192,16,128]{3,1,0,2:T(8,128)(2,1)} %copy.40), calls=%async_computation.1 | async-start | bytes 1572864 | tf_op jit(solution)/shard_map/all_to_all | solution.py:71
  28.1 2.3 %copy.43 = bf16[1,192,16,128]{3,1,0,2:T(8,128)(2,1)} copy(bf16[1,192,16,128]{3,2,1,0:T(8,128)(2,1)} %param.12) | data formatting | bytes 1572864 | tf_op args[2]
  30.4 8.2 %all-to-all-done.1 = bf16[1,192,16,128]{3,1,0,2:T(8,128)(2,1)S(1)} async-done(((bf16[1,192,16,128]{3,1,0,2:T(8,128)(2,1)}), bf16[1,192,16,128]{3,1,0,2:T(8,128)(2,1)S(1)}, u32[]{:S(2)}, u32[]{:S(2)}) %all-to-all-start.1) | async-done | bytes 786464 | tf_op jit(solution)/shard_map/all_to_all | solution.py:71
  38.6 3.5 %all-to-all-start.2 = ((bf16[1,192,16,128]{3,1,0,2:T(8,128)(2,1)}), bf16[1,192,16,128]{3,1,0,2:T(8,128)(2,1)S(1)}, u32[]{:S(2)}, u32[]{:S(2)}) async-start(bf16[1,192,16,128]{3,1,0,2:T(8,128)(2,1)} %copy.43), calls=%async_computation.2 | async-start | bytes 1572864 | tf_op jit(solution)/shard_map/all_to_all | solution.py:72
  45.3 6.5 %all-to-all-done.2 = bf16[1,192,16,128]{3,1,0,2:T(8,128)(2,1)S(1)} async-done(((bf16[1,192,16,128]{3,1,0,2:T(8,128)(2,1)}), bf16[1,192,16,128]{3,1,0,2:T(8,128)(2,1)S(1)}, u32[]{:S(2)}, u32[]{:S(2)}) %all-to-all-start.2) | async-done | bytes 786464 | tf_op jit(solution)/shard_map/all_to_all | solution.py:72
  51.8 143.6 %while.33 = (s32[]{:T(128)}, bf16[8,384,128]{2,1,0:T(8,128)(2,1)}, bf16[8,384,128]{1,2,0:T(8,128)(2,1)S(1)}, bf16[8,384,128]{1,2,0:T(8,128)(2,1)S(1)}, f32[8]{0:...) while((s32[]{:T(128)}, bf16[8,384,128]{2,1,0:T(8,128)(2,1)}, ...), condition=%wide.region_8.9_spmd, body=%wide.region_0.8_spmd.sunk | while | flops 26882248 | bytes 4764884 | solution.py:87
  53.1 16.0 %while.34 = (s32[]{:T(128)}, bf16[3,128,128]{2,1,0:T(8,128)(2,1)S(1)}, s32[3]{0:T(128)S(1)}, bf16[384,128]{0,1:T(8,128)(2,1)S(1)}, bf16[384,128]{1,0:T(8,128)(2,...) while((s32[]{:T(128)}, ...), condition=%wide.region_7.7_spmd.clone, body=%wide.region_1.6_spmd.clone.sunk | while | flops 26083076 | bytes 1811655 | solution.py:63
  62.6 0.9 multiply_reduce_fusion.2
  67.9 0.9 multiply_reduce_fusion.2
  71.1 16.0 %while.34 = (s32[]{:T(128)}, bf16[3,128,128]{2,1,0:T(8,128)(2,1)S(1)}, s32[3]{0:T(128)S(1)}, bf16[384,128]{0,1:T(8,128)(2,1)S(1)}, bf16[384,128]{1,0:T(8,128)(2,...) while((s32[]{:T(128)}, ...), condition=%wide.region_7.7_spmd.clone, body=%wide.region_1.6_spmd.clone.sunk | while | flops 26083076 | bytes 1811655 | solution.py:63
  89.0 16.0 %while.34 = (s32[]{:T(128)}, bf16[3,128,128]{2,1,0:T(8,128)(2,1)S(1)}, s32[3]{0:T(128)S(1)}, bf16[384,128]{0,1:T(8,128)(2,1)S(1)}, bf16[384,128]{1,0:T(8,128)(2,...) while((s32[]{:T(128)}, ...), condition=%wide.region_7.7_spmd.clone, body=%wide.region_1.6_spmd.clone.sunk | while | flops 26083076 | bytes 1811655 | solution.py:63
  107.0 16.0 %while.34 = (s32[]{:T(128)}, bf16[3,128,128]{2,1,0:T(8,128)(2,1)S(1)}, s32[3]{0:T(128)S(1)}, bf16[384,128]{0,1:T(8,128)(2,1)S(1)}, bf16[384,128]{1,0:T(8,128)(2,...) while((s32[]{:T(128)}, ...), condition=%wide.region_7.7_spmd.clone, body=%wide.region_1.6_spmd.clone.sunk | while | flops 26083076 | bytes 1811655 | solution.py:63
  121.8 1.0 multiply_reduce_fusion.2
  124.9 16.0 %while.34 = (s32[]{:T(128)}, bf16[3,128,128]{2,1,0:T(8,128)(2,1)S(1)}, s32[3]{0:T(128)S(1)}, bf16[384,128]{0,1:T(8,128)(2,1)S(1)}, bf16[384,128]{1,0:T(8,128)(2,...) while((s32[]{:T(128)}, ...), condition=%wide.region_7.7_spmd.clone, body=%wide.region_1.6_spmd.clone.sunk | while | flops 26083076 | bytes 1811655 | solution.py:63
  142.8 16.0 %while.34 = (s32[]{:T(128)}, bf16[3,128,128]{2,1,0:T(8,128)(2,1)S(1)}, s32[3]{0:T(128)S(1)}, bf16[384,128]{0,1:T(8,128)(2,1)S(1)}, bf16[384,128]{1,0:T(8,128)(2,...) while((s32[]{:T(128)}, ...), condition=%wide.region_7.7_spmd.clone, body=%wide.region_1.6_spmd.clone.sunk | while | flops 26083076 | bytes 1811655 | solution.py:63
  160.8 16.0 %while.34 = (s32[]{:T(128)}, bf16[3,128,128]{2,1,0:T(8,128)(2,1)S(1)}, s32[3]{0:T(128)S(1)}, bf16[384,128]{0,1:T(8,128)(2,1)S(1)}, bf16[384,128]{1,0:T(8,128)(2,...) while((s32[]{:T(128)}, ...), condition=%wide.region_7.7_spmd.clone, body=%wide.region_1.6_spmd.clone.sunk | while | flops 26083076 | bytes 1811655 | solution.py:63
  178.7 16.0 %while.34 = (s32[]{:T(128)}, bf16[3,128,128]{2,1,0:T(8,128)(2,1)S(1)}, s32[3]{0:T(128)S(1)}, bf16[384,128]{0,1:T(8,128)(2,1)S(1)}, bf16[384,128]{1,0:T(8,128)(2,...) while((s32[]{:T(128)}, ...), condition=%wide.region_7.7_spmd.clone, body=%wide.region_1.6_spmd.clone.sunk | while | flops 26083076 | bytes 1811655 | solution.py:63
  195.4 1.6 copy.59
  197.1 11.2 %all_to_all.69 = bf16[1,384,8,128]{3,2,0,1:T(8,128)(2,1)S(1)} all-to-all(bf16[1,384,8,128]{3,2,0,1:T(8,128)(2,1)S(1)} %bitcast.88), channel_id=1, replica_groups=mesh['sp'=2,'dp'=16] {'sp'}, dimensions={1} | all-to-all | bytes 1572864 | tf_op jit(solution)/shard_map/all_to_all | solution.py:91
  208.8 6.1 %fusion.12 = bf16[1,192,2048]{2,1,0:T(8,128)(2,1)} fusion(bf16[192,2048]{1,0:T(8,128)(2,1)S(1)} %reshape.130, bf16[2048,2048]{1,0:T(8,128)(2,1)} %all-gather.2.cloned.1.call-done), kind=kOutput, calls=%fused_computation.38 | convolution fusion | flops 1611005952 | bytes 9961472 | tf_op jit(solution)/shard_map/dot_general | solution.py:94
  (375 shorter events, 97.0 us)
Async XLA Ops:
  6.5 36.4 %copy-start.1 = (f32[16]{0:T(128)S(1)}, f32[16]{0:T(128)}, u32[]{:S(2)}) copy-start(f32[16]{0:T(128)} %param.13) | copy-start | bytes 196
  8.8 15.8 %all-to-all-start = ((bf16[1,192,16,128]{3,1,0,2:T(8,128)(2,1)}), bf16[1,192,16,128]{3,1,0,2:T(8,128)(2,1)S(1)}, u32[]{:S(2)}, u32[]{:S(2)}) async-start(bf16[1,192,16,128]{3,1,0,2:T(8,128)(2,1)} %copy.37), calls=%async_computation | async-start | bytes 1572864 | tf_op jit(solution)/shard_map/all_to_all | solution.py:70
  15.2 36.6 %copy-start = (f32[128]{0:T(128)S(1)}, f32[128]{0:T(128)}, u32[]{:S(2)}) copy-start(f32[128]{0:T(128)} %param.14) | copy-start | bytes 1540
  24.6 14.0 %all-to-all-start.1 = ((bf16[1,192,16,128]{3,1,0,2:T(8,128)(2,1)}), bf16[1,192,16,128]{3,1,0,2:T(8,128)(2,1)S(1)}, u32[]{:S(2)}, u32[]{:S(2)}) async-start(bf16[1,192,16,128]{3,1,0,2:T(8,128)(2,1)} %copy.40), calls=%async_computation.1 | async-start | bytes 1572864 | tf_op jit(solution)/shard_map/all_to_all | solution.py:71
  38.6 13.2 %all-to-all-start.2 = ((bf16[1,192,16,128]{3,1,0,2:T(8,128)(2,1)}), bf16[1,192,16,128]{3,1,0,2:T(8,128)(2,1)S(1)}, u32[]{:S(2)}, u32[]{:S(2)}) async-start(bf16[1,192,16,128]{3,1,0,2:T(8,128)(2,1)} %copy.43), calls=%async_computation.2 | async-start | bytes 1572864 | tf_op jit(solution)/shard_map/all_to_all | solution.py:72
  42.1 166.6 %all-gather.2.cloned.1.call-start = ((), (), s32[]{:S(2)}) async-start(), calls=%async_computation.4 | async-start | bytes 8912896 | tf_op jit(solution)/shard_map/all_gather | solution.py:96
Sparse Core Ops, SparseCore 0:
  45.1 79.5 all-gather.1
where the time goes:
time: 223 us; the launch traced here: 222 us
  loops' own time  47.4 us (21%)
  matrix products  47.1 us (21%)
  local copies, waits for them, and re-layouts  40.5 us (18%)
  other arithmetic  25.9 us (12%)
  waiting for transfers between devices  24.8 us (11%)
  between operations  13.5 us (6%)
  starting transfers between devices  11.3 us (5%)
  blocking collectives  11.2 us (5%)
    another operation x8, loops' own time, head_attention(): return lax.map(one_block, starts).reshape(length, value_head.shape[1])  46.7 us
    dot_general x24, matrix products, one_block(): mixed = jnp.dot(weights, value_head, preferred_element_type=jnp.float32)  22.8 us
    add x24, other arithmetic, one_block(): start + jnp.arange(block, dtype=jnp.int32)  15.2 us
    dynamic_slice x24, local copies, waits for them, and re-layouts, head_attention(): return lax.map(one_block, starts).reshape(length, value_head.shape[1])  14.6 us
    all_to_all x1, blocking collectives, on_device(): lax.all_to_all(attended, 'sp', split_axis=1, concat_axis=2, tiled=True)  11.2 us
    all_to_all x1, waiting for transfers between devices, on_device(): lax.all_to_all(queries, 'sp', split_axis=2, concat_axis=1, tiled=True)  9.35 us
    dot_general x24, matrix products, one_block(): jnp.dot(query_rows[:, width:], rotated_keys[:, width:].T, preferred_eleme...  9.13 us
    dot_general x24, matrix products, one_block(): jnp.dot(query_rows[:, :width], rotated_keys[:, :width].T, preferred_eleme...  9.12 us
  transfers between devices with their start and end apart: 4, of which 3 were waited for; matrix products, arithmetic and copies ran while one was open for 47% of the time, Pallas kernels for 0%

commit v1 on v0

--- a/solution.py
+++ b/solution.py
@@ -1,13 +1,18 @@
+import functools
 import math
 
 import jax
 import jax.numpy as jnp
+import numpy as np
 from jax import lax
+from jax.experimental import pallas as pl
+from jax.experimental.pallas import tpu as pltpu
 from jax.sharding import PartitionSpec as P
 
 theta_base = 500000.0
 neg_large = -1e30
 norm_eps = 1e-05
+MESH = pl.DeviceIdType.MESH
 
 
 def rotate_halves(field, positions):
@@ -99,6 +104,403 @@
     return result.reshape(seqs, tokens_here, -1)
 
 
+def rotation_tables(length, width):
+    half = width // 2
+    freqs = theta_base ** (-np.arange(half, dtype=np.float32) * np.float32(2.0) / width)
+    angle = np.arange(length, dtype=np.float32)[:, None] * freqs.astype(np.float32)[None, :]
+    cosine, sine = np.cos(angle), np.sin(angle)
+    return (
+        np.tile(cosine, (1, 4)).astype(np.float32),
+        np.tile(sine, (1, 4)).astype(np.float32),
+    )
+
+
+def turning_matrix(width):
+    half = width // 2
+    turn = np.zeros((2 * width, 2 * width), np.float32)
+    for part in range(2):
+        for j in range(half):
+            turn[part * width + half + j, part * width + j] = -1.0
+            turn[part * width + j, part * width + half + j] = 1.0
+    return turn
+
+
+def pick(table, index):
+    value = jnp.int32(table[0])
+    for i, entry in enumerate(table[1:], 1):
+        value = jnp.where(index == i, jnp.int32(entry), value)
+    return value
+
+
+def line_kernel(
+    depth_z, heads, pieces, mix_ref, q_ref, k_ref, v_ref, cos_ref, sin_ref, turn_ref, gain_ref, w_ref,
+    out_ref, far_k, far_v, wall, attended,
+    k_send, v_send, k_recv, v_recv, w_recv, up_send, down_send, side_send, core_send, extra_send, own_sem,
+):
+    s = lax.axis_index("sp")
+    d = lax.axis_index("dp")
+    c = lax.rem(d, 2)
+    y = lax.rem(d // 2, 2)
+    z = d // 4
+    tokens = q_ref.shape[0]
+    size = q_ref.shape[1] // heads
+    width = size // 2
+    columns = w_ref.shape[1]
+    rows = w_ref.shape[0] // pieces
+
+    def at(zz, yy, cc):
+        return {"sp": s, "dp": (zz * 2 + yy) * 2 + cc}
+
+    across = {"sp": 1 - s, "dp": d}
+    barrier = pltpu.get_barrier_semaphore()
+
+    def greet(target):
+        pl.semaphore_signal(barrier, inc=1, device_id=target, device_id_type=MESH)
+
+    greet(across)
+    greet(at(z, 1 - y, c))
+    greet(at(z, y, 1 - c))
+
+    @pl.when(z > 0)
+    def _():
+        greet(at(z - 1, y, c))
+
+    @pl.when(z < depth_z - 1)
+    def _():
+        greet(at(z + 1, y, c))
+
+    pl.semaphore_wait(
+        barrier,
+        3 + jnp.where(z > 0, 1, 0).astype(jnp.int32) + jnp.where(z < depth_z - 1, 1, 0).astype(jnp.int32),
+    )
+
+    def place(zz, yy, cc, q):
+        column = pl.multiple_of(((zz * 2 + yy) * 2 + cc) * columns, columns)
+        return wall.at[pl.ds(q * rows, rows), pl.ds(column, columns)]
+
+    def send(zz, yy, cc, q, sem, target, own):
+        where = place(zz, yy, cc, q)
+        return pltpu.make_async_remote_copy(
+            src_ref=w_ref.at[pl.ds(q * rows, rows), :] if own else where,
+            dst_ref=where,
+            send_sem=sem,
+            recv_sem=w_recv.at[zz, yy, cc, q],
+            device_id=target,
+            device_id_type=MESH,
+        )
+
+    near = z + 1 - 2 * lax.rem(z, 2)
+
+    def to_up(zz, q, own=False):
+        return send(zz, y, c, q, up_send.at[zz, q], at(z + 1, y, c), own)
+
+    def to_down(zz, q, own=False):
+        return send(zz, y, c, q, down_send.at[zz, q], at(z - 1, y, c), own)
+
+    def to_side(zz, q, own=False):
+        return send(zz, y, c, q, side_send.at[zz, q], at(z, 1 - y, c), own)
+
+    def to_core(zz, yy, q, own=False):
+        return send(zz, yy, c, q, core_send.at[zz, yy, q], at(z, y, 1 - c), own)
+
+    def to_near(q):
+        return send(z, 1 - y, c, q, extra_send.at[q], at(near, y, c), False)
+
+    def arrived(zz, yy, cc, q):
+        send(zz, yy, cc, q, side_send.at[0, 0], at(z, 1 - y, c), False).wait_recv()
+
+    def head_at(h):
+        return pl.ds(pl.multiple_of(h * size, size), size)
+
+    def far_copy(h, src, dst, sends, recvs):
+        return pltpu.make_async_remote_copy(
+            src_ref=src.at[:, head_at(h)],
+            dst_ref=dst.at[:, head_at(h)],
+            send_sem=sends.at[h],
+            recv_sem=recvs.at[h],
+            device_id=across,
+            device_id_type=MESH,
+        )
+
+    for q in range(pieces):
+
+        @pl.when(z > 0)
+        def _(q=q):
+            to_down(z, q, True).start()
+
+        @pl.when(z < depth_z - 1)
+        def _(q=q):
+            to_up(z, q, True).start()
+
+        to_side(z, q, True).start()
+        to_core(z, y, q, True).start()
+
+    @pl.when(s == 0)
+    def _():
+        def start(h, carry):
+            far_copy(h, k_ref, far_k, k_send, k_recv).start()
+            far_copy(h, v_ref, far_v, v_send, v_recv).start()
+            return carry
+
+        lax.fori_loop(0, heads, start, 0)
+
+    own_copy = pltpu.make_async_copy(
+        w_ref, wall.at[:, pl.ds(pl.multiple_of(d * columns, columns), columns)], own_sem
+    )
+    own_copy.start()
+
+    late = pieces // 2
+
+    def line_arrival(r, q):
+        for sign in (-1, 1):
+            zz = z + sign * r
+
+            @pl.when((zz >= 0) & (zz < depth_z))
+            def _(zz=zz, sign=sign):
+                arrived(zz, y, c, q)
+                if sign < 0:
+
+                    @pl.when(z < depth_z - 1)
+                    def _():
+                        to_up(zz, q).start()
+                else:
+
+                    @pl.when(z > 0)
+                    def _():
+                        to_down(zz, q).start()
+
+                if q < late:
+                    to_side(zz, q).start()
+                else:
+
+                    @pl.when(zz != near)
+                    def _():
+                        to_side(zz, q).start()
+
+                to_core(zz, y, q).start()
+
+    def side_arrival(r, q):
+        if r == 0:
+            arrived(z, 1 - y, c, q)
+            to_core(z, 1 - y, q).start()
+            return
+        for sign in (-1, 1):
+            zz = z + sign * r
+            here = (zz >= 0) & (zz < depth_z)
+            if q >= late:
+                here = here & (zz != near)
+
+            @pl.when(here)
+            def _(zz=zz):
+                arrived(zz, 1 - y, c, q)
+                to_core(zz, 1 - y, q).start()
+
+    def extra(q):
+        to_near(q).start()
+
+    def extra_arrival(q):
+        arrived(near, 1 - y, c, q)
+        to_core(near, 1 - y, q).start()
+
+    block_time = 4.0 * heads / 12.0
+    events = []
+    for q in range(pieces):
+        step = (q + 1) / pieces
+        for r in range(1, depth_z):
+            events.append((block_time * (r - 1 + step), functools.partial(line_arrival, r, q)))
+            events.append((block_time * (r + step) + 1.0, functools.partial(side_arrival, r, q)))
+        events.append((block_time * step + 1.0, functools.partial(side_arrival, 0, q)))
+        if q >= late:
+            events.append((block_time * (depth_z - 2) + 0.5 + 0.01 * q, functools.partial(extra, q)))
+            events.append((block_time * (depth_z - 1 + step) + 1.5, functools.partial(extra_arrival, q)))
+    events.sort(key=lambda e: e[0])
+
+    lane = lax.broadcasted_iota(jnp.int32, (tokens, size), 1)
+    visible = lax.broadcasted_iota(jnp.int32, (tokens, tokens), 0) >= lax.broadcasted_iota(
+        jnp.int32, (tokens, tokens), 1
+    )
+    my_rows = pl.ds(pl.multiple_of(s * tokens, 8), tokens)
+
+    def turned(field, table_rows):
+        crossed = jnp.dot(field, turn_ref[...], preferred_element_type=jnp.float32)
+        return field.astype(jnp.float32) * cos_ref[table_rows, :] + crossed * sin_ref[table_rows, :]
+
+    def product(a, b):
+        return lax.dot_general(a, b, (((1,), (1,)), ((), ())), preferred_element_type=jnp.float32)
+
+    def queries_of(h):
+        query = (turned(q_ref[:, head_at(h)], my_rows) * width ** (-0.5)).astype(jnp.bfloat16)
+        zero = jnp.zeros_like(query)
+        return jnp.where(lane < width, query, zero), jnp.where(lane < width, zero, query)
+
+    def finish(h, mixed):
+        scale = lax.rsqrt(jnp.mean(mixed * mixed, axis=-1, keepdims=True) + norm_eps)
+        attended[:, head_at(h)] = (mixed * scale * gain_ref[...]).astype(jnp.bfloat16)
+
+    def near_only(h):
+        key = turned(k_ref[:, head_at(h)], my_rows).astype(jnp.bfloat16)
+        maps = []
+        for query in queries_of(h):
+            scores = jnp.where(visible, product(query, key), neg_large)
+            powers = jnp.exp(scores - jnp.max(scores, axis=-1, keepdims=True))
+            maps.append((powers, jnp.sum(powers, axis=-1, keepdims=True)))
+        (first, first_sum), (second, second_sum) = maps
+        weights = first * (1.0 / first_sum) - second * (mix_ref[h] / second_sum)
+        finish(
+            h,
+            jnp.dot(weights.astype(jnp.bfloat16), v_ref[:, head_at(h)], preferred_element_type=jnp.float32),
+        )
+
+    def near_and_far(h):
+        key = turned(k_ref[:, head_at(h)], my_rows).astype(jnp.bfloat16)
+        far_key = turned(far_k[:, head_at(h)], pl.ds(0, tokens)).astype(jnp.bfloat16)
+        maps = []
+        for query in queries_of(h):
+            scores = jnp.where(visible, product(query, key), neg_large)
+            far_scores = product(query, far_key)
+            highest = jnp.maximum(
+                jnp.max(scores, axis=-1, keepdims=True), jnp.max(far_scores, axis=-1, keepdims=True)
+            )
+            powers = jnp.exp(scores - highest)
+            far_powers = jnp.exp(far_scores - highest)
+            total = jnp.sum(powers, axis=-1, keepdims=True) + jnp.sum(far_powers, axis=-1, keepdims=True)
+            maps.append((powers, far_powers, total))
+        (first, far_first, first_sum), (second, far_second, second_sum) = maps
+        one, two = 1.0 / first_sum, mix_ref[h] / second_sum
+        weights = (first * one - second * two).astype(jnp.bfloat16)
+        far_weights = (far_first * one - far_second * two).astype(jnp.bfloat16)
+        finish(
+            h,
+            jnp.dot(weights, v_ref[:, head_at(h)], preferred_element_type=jnp.float32)
+            + jnp.dot(far_weights, far_v[:, head_at(h)], preferred_element_type=jnp.float32),
+        )
+
+    def head_step(h, carry):
+        for when, action in events:
+            turn = max(0, int(when))
+            if turn < heads:
+                pl.when(h == turn)(action)
+
+        @pl.when(s == 0)
+        def _():
+            near_only(h)
+
+        @pl.when(s == 1)
+        def _():
+            far_copy(h, k_ref, far_k, k_send, k_recv).wait_recv()
+            far_copy(h, v_ref, far_v, v_send, v_recv).wait_recv()
+            near_and_far(h)
+
+        return carry
+
+    lax.fori_loop(0, heads, head_step, 0)
+    own_copy.wait()
+    for when, action in events:
+        if max(0, int(when)) >= heads:
+            action()
+
+    orders = [sorted(range(depth_z), key=lambda b: (abs(b - a), b)) for a in range(depth_z)]
+    for n in range(depth_z):
+        zz = pick([order[n] for order in orders], z)
+        for yy in (y, 1 - y):
+
+            for q in range(pieces):
+                arrived(zz, yy, 1 - c, q)
+            chip = pl.ds(pl.multiple_of((zz * 2 + yy) * 2 * columns, 2 * columns), 2 * columns)
+            out_ref[:, chip] = jnp.dot(
+                attended[...], wall[:, chip], preferred_element_type=jnp.float32
+            ).astype(out_ref.dtype)
+
+    for q in range(pieces):
+        for b in range(depth_z):
+            passed_up = (b <= z) & (z < depth_z - 1)
+            passed_down = (b >= z) & (z > 0)
+
+            @pl.when(passed_up)
+            def _(b=b):
+                to_up(b, q).wait_send()
+
+            @pl.when(passed_down)
+            def _(b=b):
+                to_down(b, q).wait_send()
+
+            if q < late:
+                to_side(b, q).wait_send()
+            else:
+
+                @pl.when(b != near)
+                def _(b=b):
+                    to_side(b, q).wait_send()
+
+            for yy in range(2):
+                to_core(b, yy, q).wait_send()
+        if q >= late:
+            to_near(q).wait_send()
+
+    @pl.when(s == 0)
+    def _():
+        def ended(h, carry):
+            far_copy(h, k_ref, far_k, k_send, k_recv).wait_send()
+            far_copy(h, v_ref, far_v, v_send, v_recv).wait_send()
+            return carry
+
+        lax.fori_loop(0, heads, ended, 0)
+
+
+def lines_of(mesh):
+    names = tuple(mesh.axis_names)
+    if names != ("sp", "dp") or mesh.shape["sp"] != 2 or mesh.shape["dp"] % 4:
+        return None
+    depth_z = mesh.shape["dp"] // 4
+    return depth_z if depth_z >= 4 and depth_z % 2 == 0 else None
+
+
+def on_line(depth_z, queries, keys, values, mix_ratio, out_gain, out_weight):
+    _, tokens, heads, size = queries.shape
+    features = heads * size
+    pieces = 4
+    cosine, sine = rotation_tables(2 * tokens, size // 2)
+    flat = [field.reshape(tokens, features) for field in (queries, keys, values)]
+    vmem = pl.BlockSpec(memory_space=pltpu.VMEM)
+    smem = pl.BlockSpec(memory_space=pltpu.SMEM)
+    dma = pltpu.SemaphoreType.DMA
+    result = pl.pallas_call(
+        functools.partial(line_kernel, depth_z, heads, pieces),
+        out_shape=jax.ShapeDtypeStruct((tokens, features), jnp.bfloat16),
+        in_specs=[smem] + [vmem] * 8,
+        out_specs=vmem,
+        scratch_shapes=[
+            pltpu.VMEM((tokens, features), jnp.bfloat16),
+            pltpu.VMEM((tokens, features), jnp.bfloat16),
+            pltpu.VMEM((features, out_weight.shape[1] * depth_z * 4), jnp.bfloat16),
+            pltpu.VMEM((tokens, features), jnp.bfloat16),
+            dma((heads,)),
+            dma((heads,)),
+            dma((heads,)),
+            dma((heads,)),
+            dma((depth_z, 2, 2, pieces)),
+            dma((depth_z, pieces)),
+            dma((depth_z, pieces)),
+            dma((depth_z, pieces)),
+            dma((depth_z, 2, pieces)),
+            dma((pieces,)),
+            dma,
+        ],
+        compiler_params=pltpu.CompilerParams(
+            collective_id=0, has_side_effects=True, vmem_limit_bytes=56 * 2**20
+        ),
+    )(
+        mix_ratio,
+        *flat,
+        jnp.asarray(cosine),
+        jnp.asarray(sine),
+        jnp.asarray(turning_matrix(size // 2), jnp.bfloat16),
+        out_gain.reshape(1, size),
+        out_weight,
+    )
+    return result.reshape(1, tokens, features)
+
+
 def solution(mesh):
     in_specs = (
         P("dp", "sp", None, None),
@@ -109,6 +511,10 @@
         P(None, "dp"),
     )
     out_specs = P("dp", "sp", None)
-    return jax.shard_map(
-        on_device, mesh=mesh, in_specs=in_specs, out_specs=out_specs, check_vma=False
-    )
+    depth_z = lines_of(mesh)
+
+    def body(queries, *rest):
+        fits = depth_z is not None and queries.shape[0] == 1 and queries.shape[1] <= 256
+        return functools.partial(on_line, depth_z)(queries, *rest) if fits else on_device(queries, *rest)
+
+    return jax.shard_map(body, mesh=mesh, in_specs=in_specs, out_specs=out_specs, check_vma=False)

time: 223 us -> 60 us (0.27)
  Pallas kernels: 0 us -> 53.9 us
  loops' own time: 47.4 us -> 0 us
  matrix products: 47.1 us -> 0 us
  local copies, waits for them, and re-layouts: 40.5 us -> 5.97 us
  other arithmetic: 25.9 us -> 0 us
  waiting for transfers between devices: 24.8 us -> 0 us
  between operations: 13.5 us -> 0.01 us
  starting transfers between devices: 11.3 us -> 0 us
  blocking collectives: 11.2 us -> 0 us
    pallas_call x0 -> x1, Pallas kernels: none -> 53.9 us  [on_line(): pl.pallas_call(functools.partial(line_kernel, depth_z, heads, pieces), ou...]
    another operation x9 -> x0, loops' own time: 47.4 us -> none  [the longest x8 46.7 us: head_attention(): return lax.map(one_block, starts).reshape(length, value_head.shape[1])]
    dot_general x73 -> x0, matrix products: 47.1 us -> none  [the longest x24 22.8 us: one_block(): mixed = jnp.dot(weights, value_head, preferred_element_type=jnp.float32)]
    all_to_all x3 -> x0, waiting for transfers between devices: 24 us -> none  [the longest x1 9.35 us: on_device(): lax.all_to_all(queries, 'sp', split_axis=2, concat_axis=1, tiled=True)]
    dynamic_slice x41 -> x0, local copies, waits for them, and re-layouts: 20 us -> none  [the longest x24 14.6 us: head_attention(): return lax.map(one_block, starts).reshape(length, value_head.shape[1])]
    add x24 -> x0, other arithmetic: 15.2 us -> none  [one_block(): start + jnp.arange(block, dtype=jnp.int32)]
    all_to_all x3 -> x0, starting transfers between devices: 11.3 us -> none  [the longest x1 4.23 us: on_device(): lax.all_to_all(queries, 'sp', split_axis=2, concat_axis=1, tiled=True)]
    all_to_all x1 -> x0, blocking collectives: 11.2 us -> none  [on_device(): lax.all_to_all(attended, 'sp', split_axis=1, concat_axis=2, tiled=True)]
  transfers between devices with their start and end apart: 4 -> 0, of which waited for: 3 -> 0; matrix products, arithmetic and copies ran while one was open for 47% -> 0% of each run, Pallas kernels for 0% -> 0%
where the time goes in v1:
time: 60 us; the launch traced here: 59.9 us
  Pallas kernels  53.9 us (90%)
  local copies, waits for them, and re-layouts  5.97 us (10%)
    pallas_call x1, Pallas kernels, on_line(): pl.pallas_call(functools.partial(line_kernel, depth_z, heads, pieces), ou...  53.9 us
    unnamed x6, local copies, waits for them, and re-layouts  4.43 us
    reshape x1, local copies, waits for them, and re-layouts, on_line(): field.reshape(tokens, features)  1.54 us

profile of v1, /device:TPU:0, one launch (start us, length us, event | category | flops | bytes accessed | tf_op | source)
XLA Modules:
  0.0 59.9 jit_solution(15916796684883513681)
XLA Ops:
  0.0 0.0 copy-start
  0.0 0.0 copy-start.1
  0.0 2.3 %copy.16 = bf16[24,8,16,128]{3,1,2,0:T(8,128)(2,1)} copy(bf16[24,8,16,128]{3,2,1,0:T(8,128)(2,1)} %bitcast.17) | data formatting | bytes 1572864
  2.3 0.0 copy-done
  2.3 0.0 copy-done.1
  2.3 1.5 %copy_bitcast_fusion = (bf16[192,2048]{1,0:T(8,128)(2,1)}, bf16[192,2048]{1,0:T(8,128)(2,1)}) fusion(bf16[24,8,16,128]{3,2,1,0:T(8,128)(2,1)S(1)} %bitcast.18, bf16[24,8,16,128]{3,2,1,0:T(8,128)(2,1)S(1)} %bitcast.19), kind=kLoop, calls=%fused_computation | loop fusion | bytes 3145728 | tf_op jit(solution)/shard_map/reshape | solution.py:463
  3.9 53.9 %shard_map.91 = bf16[192,2048]{1,0:T(8,128)(2,1)} custom-call(f32[16]{0:T(128)} %mix_ref.1, bf16[192,2048]{1,0:T(8,128)(2,1)} %bitcast.15, bf16[192,2048]{1,0:T(8,128)(2,1)} %get-tuple-element.6.k_ref, bf16[192,2048]{1,0:T(8,128)(2,1)} %get-tuple-element.5.v_ref, f32[384,128]{1,0:T(8,128)} %constant.6.clone.cos_ref, f32[384,128]{1,0:T(8,128)} %constant.7.clone.sin_ref, ...), custom_call_target="tpu_custom_call" | custom-call | tf_op jit(solution)/shard_map/pallas_call | solution.py:467
  57.8 2.1 %copy.18 = bf16[1,192,2048]{2,1,0:T(8,128)(2,1)} copy(bf16[1,192,2048]{2,1,0:T(8,128)(2,1)} %bitcast.16) | data formatting | bytes 1572864
Async XLA Ops:
  0.0 2.3 %copy-start = (bf16[1,192,16,128]{3,2,1,0:T(8,128)(2,1)S(1)}, bf16[1,192,16,128]{3,2,1,0:T(8,128)(2,1)}, u32[]{:S(2)}) copy-start(bf16[1,192,16,128]{3,2,1,0:T(8,128)(2,1)} %param.11) | copy-start | bytes 2359300
  0.0 2.3 %copy-start.1 = (bf16[1,192,16,128]{3,2,1,0:T(8,128)(2,1)S(1)}, bf16[1,192,16,128]{3,2,1,0:T(8,128)(2,1)}, u32[]{:S(2)}) copy-start(bf16[1,192,16,128]{3,2,1,0:T(8,128)(2,1)} %param.10) | copy-start | bytes 2359300

commit v2 on v1

--- a/solution.py
+++ b/solution.py
@@ -133,8 +133,8 @@
 
 
 def line_kernel(
-    depth_z, heads, pieces, mix_ref, q_ref, k_ref, v_ref, cos_ref, sin_ref, turn_ref, gain_ref, w_ref,
-    out_ref, far_k, far_v, wall, attended,
+    depth_z, heads, pieces, mix_ref, q_in, k_in, v_in, cos_in, sin_in, turn_ref, gain_ref, w_in,
+    out_ref, q_raw, k_raw, v_raw, cos_ref, sin_ref, w_ref, q_ref, k_ref, v_ref, far_k, far_v, wall, attended, in_sems,
     k_send, v_send, k_recv, v_recv, w_recv, up_send, down_send, side_send, core_send, extra_send, own_sem,
 ):
     s = lax.axis_index("sp")
@@ -152,6 +152,14 @@
         return {"sp": s, "dp": (zz * 2 + yy) * 2 + cc}
 
     across = {"sp": 1 - s, "dp": d}
+    loads = [
+        pltpu.make_async_copy(src, dst, in_sems.at[i])
+        for i, (src, dst) in enumerate(
+            [(w_in, w_ref), (k_in, k_raw), (v_in, v_raw), (q_in, q_raw), (cos_in, cos_ref), (sin_in, sin_ref)]
+        )
+    ]
+    for load in loads:
+        load.start()
     barrier = pltpu.get_barrier_semaphore()
 
     def greet(target):
@@ -173,6 +181,8 @@
         barrier,
         3 + jnp.where(z > 0, 1, 0).astype(jnp.int32) + jnp.where(z < depth_z - 1, 1, 0).astype(jnp.int32),
     )
+
+    loads[0].wait()
 
     def place(zz, yy, cc, q):
         column = pl.multiple_of(((zz * 2 + yy) * 2 + cc) * columns, columns)
@@ -235,6 +245,20 @@
         to_side(z, q, True).start()
         to_core(z, y, q, True).start()
 
+    def flatten(src, dst):
+        rows_now = math.gcd(16, tokens)
+
+        def some(i, carry):
+            part = pl.ds(pl.multiple_of(i * rows_now, rows_now), rows_now)
+            dst[part, :] = src[part, :, :].reshape(rows_now, heads * size)
+            return carry
+
+        lax.fori_loop(0, tokens // rows_now, some, 0)
+
+    for load, src, dst in ((loads[1], k_raw, k_ref), (loads[2], v_raw, v_ref), (loads[3], q_raw, q_ref)):
+        load.wait()
+        flatten(src, dst)
+
     @pl.when(s == 0)
     def _():
         def start(h, carry):
@@ -248,6 +272,8 @@
         w_ref, wall.at[:, pl.ds(pl.multiple_of(d * columns, columns), columns)], own_sem
     )
     own_copy.start()
+    loads[4].wait()
+    loads[5].wait()
 
     late = pieces // 2
 
@@ -395,21 +421,35 @@
 
     lax.fori_loop(0, heads, head_step, 0)
     own_copy.wait()
+
+    def project(zz, yy):
+        for q in range(pieces):
+            arrived(zz, yy, 1 - c, q)
+        chip = pl.ds(pl.multiple_of((zz * 2 + yy) * 2 * columns, 2 * columns), 2 * columns)
+        out_ref[:, chip] = jnp.dot(
+            attended[...], wall[:, chip], preferred_element_type=jnp.float32
+        ).astype(out_ref.dtype)
+
+    orders = [sorted(range(depth_z), key=lambda b: (abs(b - a), b)) for a in range(depth_z)]
+    sides = []
+    for a, order in enumerate(orders):
+        b = a + 1 - 2 * (a % 2)
+        sides.append([o for o in order[:-1] if o != b] + [b, order[-1]])
+    last = block_time * depth_z + 2.0
+    for n in range(depth_z):
+        zz = pick([order[n] for order in orders], z)
+        side = pick([order[n] for order in sides], z)
+        early = heads + 0.01 * n
+        line_time = max(early, block_time * n + 0.05)
+        side_time = max(early + 0.005, block_time * (n + 2 if n else 1) + 1.05)
+        if n >= depth_z - 2:
+            side_time = last + 0.01 * n
+        events.append((line_time, functools.partial(project, zz, y)))
+        events.append((side_time, functools.partial(project, side, 1 - y)))
+    events.sort(key=lambda e: e[0])
     for when, action in events:
         if max(0, int(when)) >= heads:
             action()
-
-    orders = [sorted(range(depth_z), key=lambda b: (abs(b - a), b)) for a in range(depth_z)]
-    for n in range(depth_z):
-        zz = pick([order[n] for order in orders], z)
-        for yy in (y, 1 - y):
-
-            for q in range(pieces):
-                arrived(zz, yy, 1 - c, q)
-            chip = pl.ds(pl.multiple_of((zz * 2 + yy) * 2 * columns, 2 * columns), 2 * columns)
-            out_ref[:, chip] = jnp.dot(
-                attended[...], wall[:, chip], preferred_element_type=jnp.float32
-            ).astype(out_ref.dtype)
 
     for q in range(pieces):
         for b in range(depth_z):
@@ -460,20 +500,31 @@
     features = heads * size
     pieces = 4
     cosine, sine = rotation_tables(2 * tokens, size // 2)
-    flat = [field.reshape(tokens, features) for field in (queries, keys, values)]
+    raw = [field.reshape(tokens, heads, size) for field in (queries, keys, values)]
     vmem = pl.BlockSpec(memory_space=pltpu.VMEM)
     smem = pl.BlockSpec(memory_space=pltpu.SMEM)
+    far = pl.BlockSpec(memory_space=pl.ANY)
     dma = pltpu.SemaphoreType.DMA
     result = pl.pallas_call(
         functools.partial(line_kernel, depth_z, heads, pieces),
         out_shape=jax.ShapeDtypeStruct((tokens, features), jnp.bfloat16),
-        in_specs=[smem] + [vmem] * 8,
+        in_specs=[smem, far, far, far, far, far, vmem, vmem, far],
         out_specs=vmem,
         scratch_shapes=[
+            pltpu.VMEM((tokens, heads, size), jnp.bfloat16),
+            pltpu.VMEM((tokens, heads, size), jnp.bfloat16),
+            pltpu.VMEM((tokens, heads, size), jnp.bfloat16),
+            pltpu.VMEM(cosine.shape, jnp.float32),
+            pltpu.VMEM(sine.shape, jnp.float32),
+            pltpu.VMEM(out_weight.shape, jnp.bfloat16),
+            pltpu.VMEM((tokens, features), jnp.bfloat16),
+            pltpu.VMEM((tokens, features), jnp.bfloat16),
+            pltpu.VMEM((tokens, features), jnp.bfloat16),
             pltpu.VMEM((tokens, features), jnp.bfloat16),
             pltpu.VMEM((tokens, features), jnp.bfloat16),
             pltpu.VMEM((features, out_weight.shape[1] * depth_z * 4), jnp.bfloat16),
             pltpu.VMEM((tokens, features), jnp.bfloat16),
+            dma((6,)),
             dma((heads,)),
             dma((heads,)),
             dma((heads,)),
@@ -491,7 +542,7 @@
         ),
     )(
         mix_ratio,
-        *flat,
+        *raw,
         jnp.asarray(cosine),
         jnp.asarray(sine),
         jnp.asarray(turning_matrix(size // 2), jnp.bfloat16),

time: 60 us -> 54.5 us (0.908); the launches traced: 59.9 us -> 53.5 us
  local copies, waits for them, and re-layouts: 5.97 us -> 2.09 us
  Pallas kernels: 53.9 us -> 51.4 us
    pallas_call x1, Pallas kernels: 53.9 us -> 51.4 us  [on_line(): pl.pallas_call(functools.partial(line_kernel, depth_z, heads, pieces), ou...]
    unnamed x6 -> x1, local copies, waits for them, and re-layouts: 4.43 us -> 2.09 us
    reshape x1 -> x0, local copies, waits for them, and re-layouts: 1.54 us -> none  [on_line(): field.reshape(tokens, features)]
where the time goes in v2:
time: 54.5 us; the launch traced here: 53.5 us
  Pallas kernels  51.4 us (94%)
  local copies, waits for them, and re-layouts  2.09 us (4%)
    pallas_call x1, Pallas kernels, on_line(): pl.pallas_call(functools.partial(line_kernel, depth_z, heads, pieces), ou...  51.4 us
    unnamed x1, local copies, waits for them, and re-layouts  2.09 us

profile of v2, /device:TPU:0, one launch (start us, length us, event | category | flops | bytes accessed | tf_op | source)
XLA Modules:
  0.0 53.5 jit_solution(7661457183351047293)
XLA Ops:
  0.0 51.4 %shard_map.91 = bf16[192,2048]{1,0:T(8,128)(2,1)} custom-call(f32[16]{0:T(128)} %mix_ref.1, bf16[192,16,128]{2,1,0:T(8,128)(2,1)} %bitcast.6, bf16[192,16,128]{2,1,0:T(8,128)(2,1)} %bitcast.7, bf16[192,16,128]{2,1,0:T(8,128)(2,1)} %bitcast.8, f32[384,128]{1,0:T(8,128)} %constant.6.clone.cos_in, f32[384,128]{1,0:T(8,128)} %constant.7.clone.sin_in, ...), custom_call_target="tpu_custom_call" | custom-call | tf_op jit(solution)/shard_map/pallas_call | solution.py:508
  51.4 2.1 %copy.11 = bf16[1,192,2048]{2,1,0:T(8,128)(2,1)} copy(bf16[1,192,2048]{2,1,0:T(8,128)(2,1)} %bitcast.5) | data formatting | bytes 1572864

commit v3 on v2

--- a/solution.py
+++ b/solution.py
@@ -507,7 +507,7 @@
     dma = pltpu.SemaphoreType.DMA
     result = pl.pallas_call(
         functools.partial(line_kernel, depth_z, heads, pieces),
-        out_shape=jax.ShapeDtypeStruct((tokens, features), jnp.bfloat16),
+        out_shape=pltpu.VMEM((tokens, features), jnp.bfloat16),
         in_specs=[smem, far, far, far, far, far, vmem, vmem, far],
         out_specs=vmem,
         scratch_shapes=[

time: 54.5 us -> 52.3 us (0.960)
  local copies, waits for them, and re-layouts: 2.09 us -> 0.88 us
  Pallas kernels: 51.4 us -> 50.6 us
    unnamed x1, local copies, waits for them, and re-layouts: 2.09 us -> 0.88 us
    pallas_call x1, Pallas kernels: 51.4 us -> 50.6 us  [on_line(): pl.pallas_call(functools.partial(line_kernel, depth_z, heads, pieces), ou...]
where the time goes in v3:
time: 52.3 us; the launch traced here: 51.4 us
  Pallas kernels  50.6 us (97%)
  local copies, waits for them, and re-layouts  0.88 us (2%)
    pallas_call x1, Pallas kernels, on_line(): pl.pallas_call(functools.partial(line_kernel, depth_z, heads, pieces), ou...  50.6 us

profile of v3, /device:TPU:0, one launch (start us, length us, event | category | flops | bytes accessed | tf_op | source)
XLA Modules:
  0.0 51.4 jit_solution(4953108446329238706)
XLA Ops:
  0.0 50.6 %shard_map.91 = bf16[192,2048]{1,0:T(8,128)(2,1)S(1)} custom-call(f32[16]{0:T(128)} %mix_ref.1, bf16[192,16,128]{2,1,0:T(8,128)(2,1)} %bitcast.6, bf16[192,16,128]{2,1,0:T(8,128)(2,1)} %bitcast.7, bf16[192,16,128]{2,1,0:T(8,128)(2,1)} %bitcast.8, f32[384,128]{1,0:T(8,128)} %constant.6.clone.cos_in, f32[384,128]{1,0:T(8,128)} %constant.7.clone.sin_in, ...), custom_call_target="tpu_custom_call" | custom-call | tf_op jit(solution)/shard_map/pallas_call | solution.py:508
  50.6 0.9 %copy.11 = bf16[1,192,2048]{2,1,0:T(8,128)(2,1)} copy(bf16[1,192,2048]{2,1,0:T(8,128)(2,1)S(1)} %bitcast.5) | data formatting | bytes 1572864
